TPU v7x, 32 devices: a whole 2x2x4 slice. The times are simulated.
32 devices in a mesh: ra: 8 (over z, y), cb: 4 (over x, core).
Axes of the slice: x: 2, y: 2, z: 4, core: 2. Of those that a mesh axis runs over, the one named last changes fastest.
Arguments:
- tokens: bfloat16 [512, 4096], P(None, 'cb'), may hold values from -400 to 400
- norm_gain: bfloat16 [4096], P('cb'), may hold values from 0.099609375 to 1.8984375
- w_gate: bfloat16 [4096, 11264], P('cb', 'ra'), may hold values from -0.09375 to 0.09375
- w_up: bfloat16 [4096, 11264], P('cb', 'ra'), may hold values from -0.09375 to 0.09375
- w_down: bfloat16 [11264, 4096], P('ra', 'cb'), may hold values from -0.0546875 to 0.0546875
- out_gain: bfloat16 [4096], P('cb'), may hold values from 0.099609375 to 1.8984375
Outputs:
- normed_out: bfloat16 [512, 4096], P('ra', 'cb')
All inputs are finite; a program needn't handle non-finite values.
Results may differ from a plain program's by a relative error of at most 0.0045.
Values sent between devices are 32-bit elements; how exact they have to be, the bound alone decides.
A program may use at most 64 MiB of HBM per device.

v0:
```python
import functools

import jax
import jax.numpy as jnp
from jax import lax
from jax.experimental import pallas as pl
from jax.experimental.pallas import tpu as pltpu
from jax.sharding import PartitionSpec as P

EPS = 1e-06
LANES = 128
TILE = 256
PIECES = 3
SLICES = 2
SHARES = (1, 2, 2, 1, 1, 1)
UNITS = sum(SHARES)
VMEM_BYTES = 64 * 1024 * 1024 - 64 * 1024


def plain_body(width, tokens, norm_gain, w_gate, w_up, w_down, out_gain):
    xfloat = tokens.astype(jnp.float32)
    local_sq = jnp.sum(xfloat * xfloat, axis=1)
    scaled = (xfloat * norm_gain.astype(jnp.float32)).astype(jnp.bfloat16)
    gate_part = jnp.dot(scaled, w_gate, preferred_element_type=jnp.float32)
    up_part = jnp.dot(scaled, w_up, preferred_element_type=jnp.float32)
    total_sq, gate_sum, up_sum = lax.psum((local_sq, gate_part, up_part), "cb")
    inv_in = lax.rsqrt(total_sq / width + EPS)[:, None]
    hidden = (jax.nn.silu(gate_sum * inv_in) * (up_sum * inv_in)).astype(jnp.bfloat16)
    partial_down = jnp.dot(hidden, w_down, preferred_element_type=jnp.float32)
    own_rows = tokens.shape[0] // lax.axis_size("ra")
    first_row = lax.axis_index("ra") * own_rows
    down = lax.psum_scatter(partial_down, "ra", scatter_dimension=0, tiled=True)
    residual = lax.dynamic_slice_in_dim(xfloat, first_row, own_rows, 0)
    mixed = 0.1 * residual + down
    out_sq = lax.psum(jnp.sum(mixed * mixed, axis=1), "cb")
    inv_out = lax.rsqrt(out_sq / width + EPS)[:, None]
    return (mixed * inv_out * out_gain.astype(jnp.float32)).astype(jnp.bfloat16)


def kernel(n_ra, width, subs, *refs):
    it = iter(refs)

    def take(count):
        return [next(it) for _ in range(count)]

    n = len(subs)
    tok_hbm, ng_hbm, wg_hbm, wu_hbm, wd_hbm, og_hbm, out_ref = take(7)
    tok, rest, ng, og, wgu, wd, xs, mixed, sqp, sqd, sqx, osq = take(12)
    xb, part, prec, xrec, hid, dn, yrec, zrec = [take(n) for _ in range(8)]
    ld, lw, s_d, r_d, s_x, r_x, s_h, r_h, s_y, r_y, s_z, r_z, s_o, r_o, s_q, r_q = take(16)
    depth, units = xs.shape[1], wd.shape[0]
    own = rest.shape[0]
    base = [sum(subs[:k]) for k in range(n)]
    nz = n_ra // 2
    ra, cb = lax.axis_index("ra"), lax.axis_index("cb")
    c, x = lax.rem(cb, 2), lax.div(cb, 2)
    y, z = lax.rem(ra, 2), lax.div(ra, 2)
    oc, ox, oy = 1 - c, 1 - x, 1 - y
    core_peer = (ra, x * 2 + oc)
    x_peer = (ra, ox * 2 + c)
    diag_peer = (ra, ox * 2 + oc)
    y_peer = (z * 2 + oy, cb)
    z_peers = [(lax.rem(z + d, nz) * 2 + y, cb) for d in range(1, nz)]
    mesh_id = pl.DeviceIdType.MESH
    pieces = column_pieces(2 * units)
    slices = [(i * depth // SLICES, depth // SLICES) for i in range(SLICES)]

    early = [
        pltpu.make_async_copy(tok_hbm, tok, ld.at[0]),
        pltpu.make_async_copy(ng_hbm, ng, ld.at[1]),
    ]
    weights = []
    for p, (start, size) in enumerate(pieces):
        got = []
        for i, (ref, low) in enumerate(((wg_hbm, 0), (wu_hbm, units))):
            lo, hi = max(start, low), min(start + size, low + units)
            if lo < hi:
                got.append(pltpu.make_async_copy(
                    ref.at[:, pl.ds(lo - low, hi - lo)], wgu.at[:, pl.ds(lo, hi - lo)], lw.at[p, i]))
        weights.append(got)
    late = [
        pltpu.make_async_copy(tok_hbm.at[pl.ds(pl.multiple_of(ra * own, own), own)], rest, ld.at[2]),
        pltpu.make_async_copy(og_hbm, og, ld.at[3]),
        pltpu.make_async_copy(wd_hbm, wd, ld.at[4]),
    ]
    for load in early + sum(weights, []) + late:
        load.start()

    barrier = pltpu.get_barrier_semaphore()
    peers = [core_peer, x_peer, diag_peer, y_peer] + z_peers
    for peer in peers:
        pl.semaphore_signal(barrier, inc=1, device_id=peer, device_id_type=mesh_id)

    sends = []

    def send(src, dst, s, r, peer):
        copy = pltpu.make_async_remote_copy(
            src_ref=src, dst_ref=dst, send_sem=s, recv_sem=r,
            device_id=peer, device_id_type=mesh_id)
        copy.start()
        sends.append(copy)
        return copy

    def project(k, p):
        with jax.named_scope(f"project{k}"):
            start, size = pieces[p]
            cols = pl.ds(start, size)
            got = jnp.dot(xb[k][...], wgu[:, cols], preferred_element_type=jnp.float32)
            part[k][:, :, :, cols] = got.reshape(2, 2, part[k].shape[2], size)

    def to_core(k, cols, p):
        return send(part[k].at[oc, :, :, cols], prec[k].at[:, :, cols], s_d.at[k, p], r_d.at[k, p], core_peer)

    def combine(k, copy, start, size, p):
        with jax.named_scope(f"combine{k}"):
            copy.wait_recv()
            cols = pl.ds(start, size)
            part[k][c, :, :, cols] += prec[k][:, :, cols]
            return send(part[k].at[c, ox, :, cols], xrec[k].at[:, cols], s_x.at[k, p], r_x.at[k, p], x_peer)

    def whole(k):
        for p in range(len(pieces)):
            project(k, p)
        return to_core(k, pl.ds(0, 2 * units), 0)

    def join(k, copy):
        return [combine(k, copy, 0, 2 * units, 0)]

    def activate(k, copies, inv):
        with jax.named_scope(f"activate{k}"):
            for copy in copies:
                copy.wait_recv()
            scale = inv[:part[k].shape[2], k:k + 1]
            gate = (part[k][c, x, :, :units] + xrec[k][:, :units]) * scale
            up = (part[k][c, x, :, units:] + xrec[k][:, units:]) * scale
            val = gate / (1.0 + jnp.exp(-gate)) * up
            hid[k][c, x] = val.astype(jnp.bfloat16).astype(jnp.float32)
            block = hid[k].at[c, x]
            hx = send(block, block, s_h.at[k, 0], r_h.at[k, 0], x_peer)
            h1 = send(block, block, s_h.at[k, 1], r_h.at[k, 1], core_peer)
            return hx, h1

    def forward(k, hx):
        with jax.named_scope(f"forward{k}"):
            hx.wait_recv()
            block = hid[k].at[c, ox]
            return send(block, block, s_h.at[k, 2], r_h.at[k, 2], core_peer)

    def arrived(k, h1, h2):
        h1.wait_recv()
        h2.wait_recv()

    def half(k, side):
        return hid[k][side].reshape(n_ra * subs[k] // 2, units).astype(jnp.bfloat16)

    def lower(k, h1, h2):
        with jax.named_scope(f"lower{k}"):
            pl.when(c != oy)(functools.partial(arrived, k, h1, h2))
            rows = half(k, oy)
            out = []
            for h, (start, size) in enumerate(slices):
                cols = pl.ds(start, size)
                got = jnp.dot(rows, wd[:, cols], preferred_element_type=jnp.float32)
                dn[k][oy, :, :, cols] = got.reshape(nz, subs[k], size)
                out.append(send(dn[k].at[oy, :, :, cols], yrec[k].at[:, :, cols],
                                s_y.at[k, h], r_y.at[k, h], y_peer))
            pl.when(c == oy)(functools.partial(arrived, k, h1, h2))
            got = jnp.dot(half(k, y), wd[...], preferred_element_type=jnp.float32)
            dn[k][y] = got.reshape(nz, subs[k], depth)
            return out

    def across(k, copies):
        with jax.named_scope(f"across{k}"):
            out = []
            for h, (start, size) in enumerate(slices):
                cols = pl.ds(start, size)
                copies[h].wait_recv()
                dn[k][y, :, :, cols] += yrec[k][:, :, cols]
                for d in range(1, nz):
                    out.append(send(
                        dn[k].at[y, lax.rem(z + d, nz), :, cols], zrec[k].at[d - 1, :, cols],
                        s_z.at[k, h, d - 1], r_z.at[k, h, d - 1], z_peers[d - 1]))
            return out

    def finish(k, copies):
        with jax.named_scope(f"finish{k}"):
            for copy in copies:
                copy.wait_recv()
            got = dn[k][y, z]
            for d in range(nz - 1):
                got = got + zrec[k][d]
            at = pl.ds(base[k], subs[k])
            got = mixed[at, :] + got
            mixed[at, :] = got
            osq[0, at, :] = jnp.broadcast_to(jnp.sum(got * got, axis=1, keepdims=True), (subs[k], LANES))
            return [
                send(osq.at[0, at], osq.at[i + 1, at], s_o.at[k, i], r_o.at[k, i], peer)
                for i, peer in enumerate((core_peer, x_peer, diag_peer))]

    def fill(k):
        xb[k][...] = jnp.concatenate(
            [xs[pl.ds((zz * 2 + yy) * own + base[k], subs[k]), :] for yy in range(2) for zz in range(nz)],
            axis=0).astype(jnp.bfloat16)

    def squares():
        with jax.named_scope("squares"):
            lane = lax.broadcasted_iota(jnp.int32, (own, LANES), 1)
            sqp[...] = jnp.zeros_like(sqp)
            for d in range(n_ra):
                xf = tok[pl.ds(d * own, own), :].astype(jnp.float32)
                sq = jnp.broadcast_to(jnp.sum(xf * xf, axis=1, keepdims=True), (own, LANES))
                for k in range(n):
                    at = ((d % 2) * nz + d // 2) * subs[k]
                    quarter = nz * subs[k] // 2
                    q, off = at // quarter, at % quarter
                    val = jnp.where(lane[:subs[k]] == k, sq[base[k]:base[k] + subs[k]], 0.0)
                    sqp[q // 2, q % 2, pl.ds(off, subs[k]), :] += val
            return send(sqp.at[oc], sqd, s_q.at[0], r_q.at[0], core_peer)

    with jax.named_scope("tokens"):
        for load in early:
            load.wait()
    with jax.named_scope("scale"):
        gain = ng[...].astype(jnp.float32).reshape(1, depth)
        for d in range(n_ra):
            at = pl.ds(d * own, own)
            xs[at, :] = tok[at, :].astype(jnp.float32) * gain
        fill(0)
    with jax.named_scope("enter"):
        pl.semaphore_wait(barrier, len(peers))

    a, b, h1, h2, hx, ys, zs, os = {}, {}, {}, {}, {}, {}, {}, {}
    b[0], b[1], waiting = [], [], []
    for k in range(2):
        for p, (start, size) in enumerate(pieces):
            if k == 0:
                with jax.named_scope("weights"):
                    for load in weights[p]:
                        load.wait()
            project(k, p)
            waiting.append((k, p, to_core(k, pl.ds(start, size), p)))
            if k == 0 and p == 0:
                q1 = squares()
            if len(waiting) > 1:
                kk, pp, copy = waiting.pop(0)
                b[kk].append(combine(kk, copy, *pieces[pp], pp))
            if k == 0 and p == 1:
                with jax.named_scope("share"):
                    q1.wait_recv()
                    sqp[c] += sqd[...]
                    q2 = send(sqp.at[c, ox], sqx, s_q.at[1], r_q.at[1], x_peer)
                fill(1)
    for kk, pp, copy in waiting:
        b[kk].append(combine(kk, copy, *pieces[pp], pp))
    for k in range(2, n):
        fill(k)
    for load in late:
        load.wait()
    mixed[...] = 0.1 * rest[...].astype(jnp.float32)
    for t in range(n + 3):
        if t + 2 < n:
            a[t + 2] = whole(t + 2)
        if t == 0:
            q2.wait_recv()
            inv = lax.rsqrt((sqp[c, x] + sqx[...]) / width + EPS)
        if t < n:
            hx[t], h1[t] = activate(t, b[t], inv)
        if t + 2 < n:
            b[t + 2] = join(t + 2, a[t + 2])
        if 0 <= t - 1 < n:
            h2[t - 1] = forward(t - 1, hx[t - 1])
        if t == n and n > 2:
            zs[n - 3] = across(n - 3, ys[n - 3])
        if 0 <= t - 1 < n:
            ys[t - 1] = lower(t - 1, h1[t - 1], h2[t - 1])
        if t == n and n > 3:
            os[n - 4] = finish(n - 4, zs[n - 4])
        if 0 <= t - 2 < n and t != n - 1:
            zs[t - 2] = across(t - 2, ys[t - 2])
        if 0 <= t - 3 < n and t != n - 1:
            os[t - 3] = finish(t - 3, zs[t - 3])
    with jax.named_scope("norm"):
        for k in range(n):
            for copy in os[k]:
                copy.wait_recv()
        osum = osq[0] + osq[1] + osq[2] + osq[3]
        inv_out = lax.rsqrt(osum / width + EPS)[:, :1]
        out_ref[...] = (mixed[...] * inv_out * og[...].astype(jnp.float32).reshape(1, depth)).astype(out_ref.dtype)
    with jax.named_scope("drain"):
        for copy in sends:
            copy.wait_send()


def column_pieces(total):
    tiles = total // TILE
    cuts = [tiles * i // PIECES * TILE for i in range(PIECES)] + [total]
    return [(lo, hi - lo) for lo, hi in zip(cuts[:-1], cuts[1:])]


def chunk_rows(own):
    unit = own // UNITS
    return [unit * share for share in SHARES]


def fused_body(n_ra, width, tokens, norm_gain, w_gate, w_up, w_down, out_gain):
    count, depth = tokens.shape
    units = w_down.shape[0]
    own = count // n_ra
    subs = chunk_rows(own)
    n, nz = len(subs), n_ra // 2
    f32, bf16 = jnp.float32, jnp.bfloat16
    dma = pltpu.SemaphoreType.DMA
    quarters = [n_ra * sub // 4 for sub in subs]
    most = max(quarters)
    return pl.pallas_call(
        functools.partial(kernel, n_ra, width, subs),
        out_shape=jax.ShapeDtypeStruct((own, depth), bf16),
        in_specs=[pl.BlockSpec(memory_space=pl.ANY)] * 6,
        out_specs=pl.BlockSpec(memory_space=pltpu.VMEM),
        scratch_shapes=[
            pltpu.VMEM((count, depth), bf16),
            pltpu.VMEM((own, depth), bf16),
            pltpu.VMEM((depth,), bf16),
            pltpu.VMEM((depth,), bf16),
            pltpu.VMEM((depth, 2 * units), bf16),
            pltpu.VMEM((units, depth), bf16),
            pltpu.VMEM((count, depth), f32),
            pltpu.VMEM((own, depth), f32),
            pltpu.VMEM((2, 2, most, LANES), f32),
            pltpu.VMEM((2, most, LANES), f32),
            pltpu.VMEM((most, LANES), f32),
            pltpu.VMEM((4, own, LANES), f32),
            *[pltpu.VMEM((n_ra * sub, depth), bf16) for sub in subs],
            *[pltpu.VMEM((2, 2, quarter, 2 * units), f32) for quarter in quarters],
            *[pltpu.VMEM((2, quarter, 2 * units), f32) for quarter in quarters],
            *[pltpu.VMEM((quarter, 2 * units), f32) for quarter in quarters],
            *[pltpu.VMEM((2, 2, quarter, units), f32) for quarter in quarters],
            *[pltpu.VMEM((2, nz, sub, depth), f32) for sub in subs],
            *[pltpu.VMEM((nz, sub, depth), f32) for sub in subs],
            *[pltpu.VMEM((nz - 1, sub, depth), f32) for sub in subs],
            dma((5,)),
            dma((PIECES, 2)),
            *[dma((n, PIECES)) for _ in range(4)],
            *[dma((n, 3)) for _ in range(2)],
            *[dma((n, SLICES)) for _ in range(2)],
            *[dma((n, SLICES, nz - 1)) for _ in range(2)],
            *[dma((n, 3)) for _ in range(2)],
            *[dma((2,)) for _ in range(2)],
        ],
        compiler_params=pltpu.CompilerParams(
            collective_id=0, has_side_effects=True, vmem_limit_bytes=VMEM_BYTES),
    )(tokens, norm_gain, w_gate, w_up, w_down, out_gain)


def solution(mesh):
    n_ra, n_cb = mesh.shape["ra"], mesh.shape["cb"]

    def body(*args):
        tokens, w_down = args[0], args[4]
        count, depth = tokens.shape
        units = w_down.shape[0]
        width = depth * n_cb
        tiled = (
            n_cb == 4 and n_ra % 4 == 0 and n_ra > 2
            and count % (n_ra * UNITS * 8) == 0 and units % LANES == 0 and depth % TILE == 0
            and depth % (SLICES * LANES) == 0)
        if tiled:
            return fused_body(n_ra, width, *args)
        return plain_body(width, *args)

    return jax.shard_map(
        body,
        mesh=mesh,
        in_specs=(P(None, "cb"), P("cb"), P("cb", "ra"), P("cb", "ra"), P("ra", "cb"), P("cb")),
        out_specs=P("ra", "cb"),
        check_vma=False,
    )
```

profile of v0, /device:TPU:0, one launch (start us, length us, event | category | flops | bytes accessed | tf_op | source)
XLA Modules:
  0.0 73.5 jit_solution(2167521530069878375)
XLA Ops:
  0.0 71.9 %shard_map.64 = bf16[64,1024]{1,0:T(8,128)(2,1)} custom-call(bf16[512,1024]{1,0:T(8,128)(2,1)} %refs_0_.1, bf16[1024]{0:T(1024)(128)(2,1)} %refs_1_.1, bf16[1024,1408]{1,0:T(8,128)(2,1)} %refs_2_.1, bf16[1024,1408]{1,0:T(8,128)(2,1)} %refs_3_.1, bf16[1408,1024]{1,0:T(8,128)(2,1)} %refs_4_.1, bf16[1024]{0:T(1024)(128)(2,1)} %refs_5_.1), custom_call_target="tpu_custom_call" | custom-call | tf_op jit(solution)/shard_map/pallas_call | solution.py:315
  71.9 1.6 %copy.8 = bf16[64,1024]{1,0:T(8,128)(2,1)} copy(bf16[64,1024]{1,0:T(8,128)(2,1)} %shard_map.64) | data formatting | bytes 262144
where the time goes:
time: 73.6 us; the launch traced here: 73.5 us
  Pallas kernels  71.9 us (98%)
  local copies, waits for them, and re-layouts  1.57 us (2%)
    pallas_call x1, Pallas kernels, fused_body(): pl.pallas_call(functools.partial(kernel, n_ra, width, subs), out_shape=ja...  71.9 us
    unnamed x1, local copies, waits for them, and re-layouts  1.57 us

commit v1 on v0

--- a/solution.py
+++ b/solution.py
@@ -14,7 +14,7 @@
 SLICES = 2
 SHARES = (1, 2, 2, 1, 1, 1)
 UNITS = sum(SHARES)
-VMEM_BYTES = 64 * 1024 * 1024 - 64 * 1024
+VMEM_BYTES = 63 * 1024 * 1024 - 64 * 1024
 
 
 def plain_body(width, tokens, norm_gain, w_gate, w_up, w_down, out_gain):
@@ -314,7 +314,7 @@
     most = max(quarters)
     return pl.pallas_call(
         functools.partial(kernel, n_ra, width, subs),
-        out_shape=jax.ShapeDtypeStruct((own, depth), bf16),
+        out_shape=pltpu.VMEM((own, depth), bf16),
         in_specs=[pl.BlockSpec(memory_space=pl.ANY)] * 6,
         out_specs=pl.BlockSpec(memory_space=pltpu.VMEM),
         scratch_shapes=[

time: 73.6 us -> 72.1 us (0.980)
  local copies, waits for them, and re-layouts: 1.57 us -> 0.66 us
    unnamed x1, local copies, waits for them, and re-layouts: 1.57 us -> 0.66 us
where the time goes in v1:
time: 72.1 us; the launch traced here: 71.9 us
  Pallas kernels  71.3 us (99%)
    pallas_call x1, Pallas kernels, fused_body(): pl.pallas_call(functools.partial(kernel, n_ra, width, subs), out_shape=pl...  71.3 us

profile of v1, /device:TPU:0, one launch (start us, length us, event | category | flops | bytes accessed | tf_op | source)
XLA Modules:
  0.0 71.9 jit_solution(4357997220739711122)
XLA Ops:
  0.0 71.3 %shard_map.64 = bf16[64,1024]{1,0:T(8,128)(2,1)S(1)} custom-call(bf16[512,1024]{1,0:T(8,128)(2,1)} %refs_0_.1, bf16[1024]{0:T(1024)(128)(2,1)} %refs_1_.1, bf16[1024,1408]{1,0:T(8,128)(2,1)} %refs_2_.1, bf16[1024,1408]{1,0:T(8,128)(2,1)} %refs_3_.1, bf16[1408,1024]{1,0:T(8,128)(2,1)} %refs_4_.1, bf16[1024]{0:T(1024)(128)(2,1)} %refs_5_.1), custom_call_target="tpu_custom_call" | custom-call | tf_op jit(solution)/shard_map/pallas_call | solution.py:315
  71.3 0.7 copy.8

commit v2 on v1

v2 whole, which is shorter than its diff:
```python
import functools

import jax
import jax.numpy as jnp
from jax import lax
from jax.experimental import pallas as pl
from jax.experimental.pallas import tpu as pltpu
from jax.sharding import PartitionSpec as P

EPS = 1e-06
LANES = 128
TILE = 256
WHOLE, OUTER, INNER = "whole", "outer", "inner"
CHUNKS = (
    (1, WHOLE), (2, WHOLE), (1, WHOLE), (1, WHOLE), (1, WHOLE), (1, OUTER), (1, INNER), (1, OUTER), (1, INNER))
UNITS = sum(share if owners == WHOLE else share / 2 for share, owners in CHUNKS)
FIRST_CUTS = (0, 1, 3, 5, 8)
SECOND_CUTS = (0, 3, 7)
VMEM_BYTES = 63 * 1024 * 1024 - 64 * 1024
STEPS = (
    "P2 A0 P3 P4", "J2 J3 A1 J4", "P5 F0 L0 A2", "J5 P6 Y0 A3", "J6 P7 F1 L1", "Z0 A4 J7 P8",
    "F2 L2 A5 J8", "Y1 F3 L3 A6", "Y2 F4 L4 A7", "F5 Y3 L5 A8", "Z1 F6 F7 Y4", "L6 F8 L7 Y5",
    "Z2 L8 Z3 Y6", "Y7 Z4 Y8 Z5", "Z6 Z7 Z8",
)
SLICES = (1, 1, 1, 1, 1, 2, 2, 2, 4)


def plain_body(width, tokens, norm_gain, w_gate, w_up, w_down, out_gain):
    xfloat = tokens.astype(jnp.float32)
    local_sq = jnp.sum(xfloat * xfloat, axis=1)
    scaled = (xfloat * norm_gain.astype(jnp.float32)).astype(jnp.bfloat16)
    gate_part = jnp.dot(scaled, w_gate, preferred_element_type=jnp.float32)
    up_part = jnp.dot(scaled, w_up, preferred_element_type=jnp.float32)
    total_sq, gate_sum, up_sum = lax.psum((local_sq, gate_part, up_part), "cb")
    inv_in = lax.rsqrt(total_sq / width + EPS)[:, None]
    hidden = (jax.nn.silu(gate_sum * inv_in) * (up_sum * inv_in)).astype(jnp.bfloat16)
    partial_down = jnp.dot(hidden, w_down, preferred_element_type=jnp.float32)
    own_rows = tokens.shape[0] // lax.axis_size("ra")
    first_row = lax.axis_index("ra") * own_rows
    down = lax.psum_scatter(partial_down, "ra", scatter_dimension=0, tiled=True)
    residual = lax.dynamic_slice_in_dim(xfloat, first_row, own_rows, 0)
    mixed = 0.1 * residual + down
    out_sq = lax.psum(jnp.sum(mixed * mixed, axis=1), "cb")
    inv_out = lax.rsqrt(out_sq / width + EPS)[:, None]
    return (mixed * inv_out * out_gain.astype(jnp.float32)).astype(jnp.bfloat16)


def column_pieces(k, total):
    cuts = FIRST_CUTS if k == 0 else SECOND_CUTS if k == 1 else (0,)
    edges = [cut * TILE for cut in cuts] + [total]
    return [(lo, hi - lo) for lo, hi in zip(edges[:-1], edges[1:])]


def chunk_layout(own, nz):
    zs = {WHOLE: list(range(nz)), OUTER: [0, nz - 1], INNER: list(range(1, nz - 1))}
    unit = own // int(UNITS)
    out, at = [], 0
    for share, owners in CHUNKS:
        out.append((at, unit * share, zs[owners]))
        at += unit * share if owners in (WHOLE, INNER) else 0
    return out


def semaphore_slots(total):
    n = len(CHUNKS)
    keys = ["rows", "rest", "gain", "out_gain", "down"]
    keys += [("weights", p) for p in range(len(FIRST_CUTS))]
    for k in range(n):
        keys += [("dr", k, p) for p in range(len(column_pieces(k, total)))]
        keys += [("xr", k), ("hr", k), ("fr", k), ("zr", k)] + [("yr", k, h) for h in range(SLICES[k])]
    keys += [("qr", 0), ("qr", 1), "or", "os"]
    for ring, depth in RINGS.items():
        keys += [(ring, i) for i in range(depth)]
    return {key: i for i, key in enumerate(keys)}


RINGS = {"ds": 3, "xs": 4, "hs": 4, "cs": 2, "fs": 2, "ys": 3, "zs": 3, "qs": 1}


def kernel(n_ra, width, layout, *refs):
    it = iter(refs)

    def take(count):
        return [next(it) for _ in range(count)]

    n = len(layout)
    tok_hbm, ng_hbm, wg_hbm, wu_hbm, wd_hbm, og_hbm, out_ref = take(7)
    first, tok, ng, og, wgu, wd, xs, mixed, sqp, sqd, sqx, osq = take(12)
    xb, part, prec, xrec, hid, dn, yrec, zrec = [take(n) for _ in range(8)]
    (sems,) = take(1)
    depth, units = xs.shape[1], wd.shape[0]
    own = mixed.shape[0]
    nz = n_ra // 2
    ra, cb = lax.axis_index("ra"), lax.axis_index("cb")
    c, x = lax.rem(cb, 2), lax.div(cb, 2)
    y, z = lax.rem(ra, 2), lax.div(ra, 2)
    oc, ox, oy = 1 - c, 1 - x, 1 - y
    core_peer = (ra, x * 2 + oc)
    x_peer = (ra, ox * 2 + c)
    diag_peer = (ra, ox * 2 + oc)
    y_peer = (z * 2 + oy, cb)
    mesh_id = pl.DeviceIdType.MESH
    slots = semaphore_slots(2 * units)
    head = layout[0][1]

    def sem(*key):
        return sems.at[slots[key if len(key) > 1 else key[0]]]

    early = [
        pltpu.make_async_copy(tok_hbm.at[pl.ds(d * own, head)], first.at[pl.ds(d * head, head)], sem("rows"))
        for d in range(n_ra)
    ] + [pltpu.make_async_copy(ng_hbm, ng, sem("gain"))]
    weights = []
    for p, (start, size) in enumerate(column_pieces(0, 2 * units)):
        got = []
        for ref, low in ((wg_hbm, 0), (wu_hbm, units)):
            lo, hi = max(start, low), min(start + size, low + units)
            if lo < hi:
                got.append(pltpu.make_async_copy(
                    ref.at[:, pl.ds(lo - low, hi - lo)], wgu.at[:, pl.ds(lo, hi - lo)], sem("weights", p)))
        weights.append(got)
    whole_tok = pltpu.make_async_copy(tok_hbm, tok, sem("rest"))
    late = [
        pltpu.make_async_copy(og_hbm, og, sem("out_gain")),
        pltpu.make_async_copy(wd_hbm, wd, sem("down")),
    ]
    for load in early + sum(weights[:3], []) + [whole_tok] + sum(weights[3:], []) + late:
        load.start()

    barrier = pltpu.get_barrier_semaphore()
    peers = [core_peer, x_peer, diag_peer, y_peer] + [(lax.rem(z + d, nz) * 2 + y, cb) for d in range(1, nz)]
    for peer in peers:
        pl.semaphore_signal(barrier, inc=1, device_id=peer, device_id_type=mesh_id)

    used = {ring: [None] * size for ring, size in RINGS.items()}
    turn = {ring: 0 for ring in RINGS}

    def slot_of(ring, leave):
        i = turn[ring] % RINGS[ring]
        turn[ring] += 1
        if used[ring][i] is not None:
            used[ring][i]()
        used[ring][i] = leave
        return sem(ring, i)

    def remote(src, dst, s, r, peer):
        return pltpu.make_async_remote_copy(
            src_ref=src, dst_ref=dst, send_sem=s, recv_sem=r, device_id=peer, device_id_type=mesh_id)

    def send(src, dst, ring, r, peer):
        made = []
        s = slot_of(ring, lambda: made[0].wait_send())
        made.append(remote(src, dst, s, r, peer))
        made[0].start()
        return made[0]

    def wait_bytes(ref, s):
        pltpu.make_async_copy(ref, ref, s).wait()

    def project(k, p=0):
        with jax.named_scope(f"project{k}"):
            start, size = column_pieces(k, 2 * units)[p]
            cols = pl.ds(start, size)
            got = jnp.dot(xb[k][...], wgu[:, cols], preferred_element_type=jnp.float32)
            part[k][:, :, :, cols] = got.reshape(2, 2, part[k].shape[2], size)

    def to_core(k, p=0):
        cols = pl.ds(*column_pieces(k, 2 * units)[p])
        return send(part[k].at[oc, :, :, cols], prec[k].at[:, :, cols], "ds", sem("dr", k, p), core_peer)

    leaving = {}

    def combine(k, p, copy):
        with jax.named_scope(f"combine{k}"):
            copy.wait_recv()
            cols = pl.ds(*column_pieces(k, 2 * units)[p])
            part[k][c, :, :, cols] += prec[k][:, :, cols]
            if k not in leaving:
                leaving[k] = slot_of("xs", lambda: wait_bytes(xrec[k], leaving[k]))
            remote(part[k].at[c, ox, :, cols], xrec[k].at[:, cols], leaving[k], sem("xr", k), x_peer).start()

    def activate(k, inv):
        with jax.named_scope(f"activate{k}"):
            wait_bytes(xrec[k], sem("xr", k))
            scale = inv[:part[k].shape[2], k:k + 1]
            gate = (part[k][c, x, :, :units] + xrec[k][:, :units]) * scale
            up = (part[k][c, x, :, units:] + xrec[k][:, units:]) * scale
            val = gate / (1.0 + jnp.exp(-gate)) * up
            hid[k][c, x] = val.astype(jnp.bfloat16).astype(jnp.float32)
            block = hid[k].at[c, x]
            hx = send(block, block, "hs", sem("hr", k), x_peer)
            send(block, block, "cs", sem("fr", k), core_peer)
            return hx

    def forward(k, hx):
        with jax.named_scope(f"forward{k}"):
            hx.wait_recv()
            block = hid[k].at[c, ox]
            send(block, block, "fs", sem("fr", k), core_peer)

    def lower(k):
        with jax.named_scope(f"lower{k}"):
            wait_bytes(hid[k].at[oc], sem("fr", k))
            _, sub, zs = layout[k]
            rows = hid[k][...].reshape(2 * len(zs) * sub, units).astype(jnp.bfloat16)
            s = slot_of("ys", lambda: wait_bytes(yrec[k], s))
            for h, (start, size) in enumerate(slices(k)):
                cols = pl.ds(start, size)
                got = jnp.dot(rows, wd[:, cols], preferred_element_type=jnp.float32)
                dn[k][:, :, :, cols] = got.reshape(2, len(zs), sub, size)
                remote(dn[k].at[oy, :, :, cols], yrec[k].at[:, :, cols], s, sem("yr", k, h), y_peer).start()

    def slices(k):
        return [(h * depth // SLICES[k], depth // SLICES[k]) for h in range(SLICES[k])]

    def owns(zs):
        return functools.reduce(jnp.logical_or, [z == zz for zz in zs])

    def across(k):
        with jax.named_scope(f"across{k}"):
            _, sub, zs = layout[k]

            def leave():
                if len(zs) == nz:
                    wait_bytes(zrec[k], s)
                else:
                    mine = owns(zs)
                    pl.when(mine)(lambda: wait_bytes(zrec[k].at[pl.ds(0, len(zs) - 1)], s))
                    pl.when(jnp.logical_not(mine))(lambda: wait_bytes(zrec[k].at[pl.ds(0, len(zs))], s))

            s = slot_of("zs", leave)
            for h, (start, size) in enumerate(slices(k)):
                cols = pl.ds(start, size)
                wait_bytes(yrec[k].at[:, :, cols], sem("yr", k, h))
                dn[k][y, :, :, cols] += yrec[k][:, :, cols]
                for j, zz in enumerate(zs):
                    @pl.when(z != zz)
                    def _(j=j, zz=zz, cols=cols):
                        slot = lax.rem(zz - z + nz, nz) - 1
                        remote(dn[k].at[y, j, :, cols], zrec[k].at[slot, :, cols], s, sem("zr", k),
                               (zz * 2 + y, cb)).start()

    def finish(k):
        base, sub, zs = layout[k]

        def run():
            wait_bytes(zrec[k], sem("zr", k))
            at = pl.ds(base, sub)
            index = z if len(zs) == nz else lax.div(z, nz - 1) if zs[0] == 0 else z - zs[0]
            got = dn[k][y, index]
            for d in range(nz - 1):
                got = got + zrec[k][d]
            got = mixed[at, :] + got
            mixed[at, :] = got
            osq[0, at, :] = jnp.broadcast_to(jnp.sum(got * got, axis=1, keepdims=True), (sub, LANES))
            for i, peer in enumerate((core_peer, x_peer, diag_peer)):
                remote(osq.at[0, at], osq.at[i + 1, at], sem("os"), sem("or"), peer).start()

        with jax.named_scope(f"finish{k}"):
            if len(zs) == nz:
                run()
            else:
                pl.when(owns(zs))(run)

    def fill(k):
        base, sub, zs = layout[k]
        xb[k][...] = jnp.concatenate(
            [xs[pl.ds((zz * 2 + yy) * own + base, sub), :] for yy in range(2) for zz in zs], axis=0).astype(jnp.bfloat16)

    def squares():
        with jax.named_scope("squares"):
            lane = lax.broadcasted_iota(jnp.int32, (own, LANES), 1)
            sqp[...] = jnp.zeros_like(sqp)
            for d in range(n_ra):
                xf = tok[pl.ds(d * own, own), :].astype(jnp.float32)
                sq = jnp.broadcast_to(jnp.sum(xf * xf, axis=1, keepdims=True), (own, LANES))
                for k, (base, sub, zs) in enumerate(layout):
                    if d // 2 not in zs:
                        continue
                    at = ((d % 2) * len(zs) + zs.index(d // 2)) * sub
                    quarter = len(zs) * sub // 2
                    q, off = at // quarter, at % quarter
                    val = jnp.where(lane[:sub] == k, sq[base:base + sub], 0.0)
                    sqp[q // 2, q % 2, pl.ds(off, sub), :] += val
            return send(sqp.at[oc], sqd, "qs", sem("qr", 0), core_peer)

    with jax.named_scope("tokens"):
        wait_bytes(first, sem("rows"))
        early[-1].wait()
    with jax.named_scope("scale"):
        gain = ng[...].astype(jnp.float32).reshape(1, depth)
        lead = first[...].astype(jnp.float32) * gain
        _, sub, zs = layout[0]
        xb[0][...] = jnp.concatenate(
            [lead[(zz * 2 + yy) * sub:(zz * 2 + yy + 1) * sub] for yy in range(2) for zz in zs], axis=0).astype(jnp.bfloat16)

    waiting = []

    def settle(left):
        while len(waiting) > left:
            k, p, copy = waiting.pop(0)
            combine(k, p, copy)

    for p, piece in enumerate(column_pieces(0, 2 * units)):
        with jax.named_scope("weights"):
            wait_bytes(wgu.at[:, pl.ds(*piece)], sem("weights", p))
        project(0, p)
        if p == 0:
            with jax.named_scope("enter"):
                pl.semaphore_wait(barrier, len(peers))
        waiting.append((0, p, to_core(0, p)))
        settle(2)
    with jax.named_scope("rest"):
        whole_tok.wait()
    q1 = squares()
    settle(1)
    with jax.named_scope("fill"):
        for d in range(n_ra):
            at = pl.ds(d * own, own)
            xs[at, :] = tok[at, :].astype(jnp.float32) * gain
        fill(1)
    settle(0)
    with jax.named_scope("share"):
        q1.wait_recv()
        sqp[c] += sqd[...]
        q2 = send(sqp.at[c, ox], sqx, "qs", sem("qr", 1), x_peer)
    for p in range(len(column_pieces(1, 2 * units))):
        project(1, p)
        waiting.append((1, p, to_core(1, p)))
        settle(1)
    settle(0)
    for k in range(2, n):
        fill(k)
    for load in late:
        load.wait()
    mixed[...] = 0.1 * tok[pl.ds(pl.multiple_of(ra * own, own), own), :].astype(jnp.float32)

    inv, sent, hx = None, {}, {}
    for step in [step for group in STEPS for step in group.split()]:
        what, k = step[0], int(step[1:])
        if what == "P":
            project(k)
            sent[k] = to_core(k)
        elif what == "J":
            combine(k, 0, sent[k])
        elif what == "A":
            if inv is None:
                q2.wait_recv()
                inv = lax.rsqrt((sqp[c, x] + sqx[...]) / width + EPS)
            hx[k] = activate(k, inv)
        elif what == "F":
            forward(k, hx[k])
        elif what == "L":
            lower(k)
        elif what == "Y":
            across(k)
        else:
            finish(k)
    with jax.named_scope("norm"):
        wait_bytes(osq.at[pl.ds(1, 3)], sem("or"))
        osum = osq[0] + osq[1] + osq[2] + osq[3]
        inv_out = lax.rsqrt(osum / width + EPS)[:, :1]
        out_ref[...] = (mixed[...] * inv_out * og[...].astype(jnp.float32).reshape(1, depth)).astype(out_ref.dtype)
    with jax.named_scope("drain"):
        for waits in used.values():
            for leave in waits:
                if leave is not None:
                    leave()
        wait_bytes(osq.at[pl.ds(1, 3)], sem("os"))


def fused_body(n_ra, width, tokens, norm_gain, w_gate, w_up, w_down, out_gain):
    count, depth = tokens.shape
    units = w_down.shape[0]
    own = count // n_ra
    nz = n_ra // 2
    layout = chunk_layout(own, nz)
    f32, bf16 = jnp.float32, jnp.bfloat16
    rows = [2 * len(zs) * sub for _, sub, zs in layout]
    quarters = [count // 4 for count in rows]
    most = max(quarters)
    return pl.pallas_call(
        functools.partial(kernel, n_ra, width, layout),
        out_shape=pltpu.VMEM((own, depth), bf16),
        in_specs=[pl.BlockSpec(memory_space=pl.ANY)] * 6,
        out_specs=pl.BlockSpec(memory_space=pltpu.VMEM),
        scratch_shapes=[
            pltpu.VMEM((rows[0], depth), bf16),
            pltpu.VMEM((count, depth), bf16),
            pltpu.VMEM((depth,), bf16),
            pltpu.VMEM((depth,), bf16),
            pltpu.VMEM((depth, 2 * units), bf16),
            pltpu.VMEM((units, depth), bf16),
            pltpu.VMEM((count, depth), f32),
            pltpu.VMEM((own, depth), f32),
            pltpu.VMEM((2, 2, most, LANES), f32),
            pltpu.VMEM((2, most, LANES), f32),
            pltpu.VMEM((most, LANES), f32),
            pltpu.VMEM((4, own, LANES), f32),
            *[pltpu.VMEM((count, depth), bf16) for count in rows],
            *[pltpu.VMEM((2, 2, quarter, 2 * units), f32) for quarter in quarters],
            *[pltpu.VMEM((2, quarter, 2 * units), f32) for quarter in quarters],
            *[pltpu.VMEM((quarter, 2 * units), f32) for quarter in quarters],
            *[pltpu.VMEM((2, 2, quarter, units), f32) for quarter in quarters],
            *[pltpu.VMEM((2, len(zs), sub, depth), f32) for _, sub, zs in layout],
            *[pltpu.VMEM((len(zs), sub, depth), f32) for _, sub, zs in layout],
            *[pltpu.VMEM((nz - 1, sub, depth), f32) for _, sub, _ in layout],
            pltpu.SemaphoreType.DMA((len(semaphore_slots(2 * units)),)),
        ],
        compiler_params=pltpu.CompilerParams(
            collective_id=0, has_side_effects=True, vmem_limit_bytes=VMEM_BYTES),
    )(tokens, norm_gain, w_gate, w_up, w_down, out_gain)


def solution(mesh):
    n_ra, n_cb = mesh.shape["ra"], mesh.shape["cb"]

    def body(*args):
        tokens, w_down = args[0], args[4]
        count, depth = tokens.shape
        units = w_down.shape[0]
        width = depth * n_cb
        tiled = (
            n_cb == 4 and n_ra == 8
            and count % (n_ra * int(UNITS) * 8) == 0 and units % LANES == 0 and depth % TILE == 0
            and depth % (max(SLICES) * LANES) == 0 and 2 * units > TILE * max(FIRST_CUTS + SECOND_CUTS))
        if tiled:
            return fused_body(n_ra, width, *args)
        return plain_body(width, *args)

    return jax.shard_map(
        body,
        mesh=mesh,
        in_specs=(P(None, "cb"), P("cb"), P("cb", "ra"), P("cb", "ra"), P("ra", "cb"), P("cb")),
        out_specs=P("ra", "cb"),
        check_vma=False,
    )
```

time: 72.1 us -> 68.8 us (0.954)
  Pallas kernels: 71.3 us -> 68 us
    pallas_call x1, Pallas kernels: 71.3 us -> 68 us  [fused_body(): pl.pallas_call(functools.partial(kernel, n_ra, width, layout), out_shape=...]
where the time goes in v2:
time: 68.8 us; the launch traced here: 68.6 us
  Pallas kernels  68 us (99%)
    pallas_call x1, Pallas kernels, fused_body(): pl.pallas_call(functools.partial(kernel, n_ra, width, layout), out_shape=...  68 us

profile of v2, /device:TPU:0, one launch (start us, length us, event | category | flops | bytes accessed | tf_op | source)
XLA Modules:
  0.0 68.6 jit_solution(6158618515690865108)
XLA Ops:
  0.0 68.0 %shard_map.64 = bf16[64,1024]{1,0:T(8,128)(2,1)S(1)} custom-call(bf16[512,1024]{1,0:T(8,128)(2,1)} %refs_0_.1, bf16[1024]{0:T(1024)(128)(2,1)} %refs_1_.1, bf16[1024,1408]{1,0:T(8,128)(2,1)} %refs_2_.1, bf16[1024,1408]{1,0:T(8,128)(2,1)} %refs_3_.1, bf16[1408,1024]{1,0:T(8,128)(2,1)} %refs_4_.1, bf16[1024]{0:T(1024)(128)(2,1)} %refs_5_.1), custom_call_target="tpu_custom_call" | custom-call | tf_op jit(solution)/shard_map/pallas_call | solution.py:382
  68.0 0.7 copy.8

commit v3 on v2

--- a/solution.py
+++ b/solution.py
@@ -12,7 +12,7 @@
 TILE = 256
 WHOLE, OUTER, INNER = "whole", "outer", "inner"
 CHUNKS = (
-    (1, WHOLE), (2, WHOLE), (1, WHOLE), (1, WHOLE), (1, WHOLE), (1, OUTER), (1, INNER), (1, OUTER), (1, INNER))
+    (1, WHOLE), (2, WHOLE), (1, WHOLE), (1, WHOLE), (1, WHOLE), (1, OUTER), (1, OUTER), (1, INNER), (1, INNER))
 UNITS = sum(share if owners == WHOLE else share / 2 for share, owners in CHUNKS)
 FIRST_CUTS = (0, 1, 3, 5, 8)
 SECOND_CUTS = (0, 3, 7)
@@ -22,7 +22,7 @@
     "F2 L2 A5 J8", "Y1 F3 L3 A6", "Y2 F4 L4 A7", "F5 Y3 L5 A8", "Z1 F6 F7 Y4", "L6 F8 L7 Y5",
     "Z2 L8 Z3 Y6", "Y7 Z4 Y8 Z5", "Z6 Z7 Z8",
 )
-SLICES = (1, 1, 1, 1, 1, 2, 2, 2, 4)
+SLICES = (1, 1, 1, 1, 1, 2, 2, 2, 2)
 
 
 def plain_body(width, tokens, norm_gain, w_gate, w_up, w_down, out_gain):
@@ -54,10 +54,11 @@
 def chunk_layout(own, nz):
     zs = {WHOLE: list(range(nz)), OUTER: [0, nz - 1], INNER: list(range(1, nz - 1))}
     unit = own // int(UNITS)
-    out, at = [], 0
+    out, at = [], [0] * nz
     for share, owners in CHUNKS:
-        out.append((at, unit * share, zs[owners]))
-        at += unit * share if owners in (WHOLE, INNER) else 0
+        out.append((at[zs[owners][0]], unit * share, zs[owners]))
+        for z in zs[owners]:
+            at[z] += unit * share
     return out
 
 
@@ -309,7 +310,7 @@
             with jax.named_scope("enter"):
                 pl.semaphore_wait(barrier, len(peers))
         waiting.append((0, p, to_core(0, p)))
-        settle(2)
+        settle(1 if p == 2 else 2)
     with jax.named_scope("rest"):
         whole_tok.wait()
     q1 = squares()

time: 68.8 us -> 67.5 us (0.981)
  Pallas kernels: 68 us -> 66.7 us
    pallas_call x1, Pallas kernels: 68 us -> 66.7 us  [fused_body(): pl.pallas_call(functools.partial(kernel, n_ra, width, layout), out_shape=...]
where the time goes in v3:
time: 67.5 us; the launch traced here: 67.4 us
  Pallas kernels  66.7 us (99%)
    pallas_call x1, Pallas kernels, fused_body(): pl.pallas_call(functools.partial(kernel, n_ra, width, layout), out_shape=...  66.7 us

profile of v3, /device:TPU:0, one launch (start us, length us, event | category | flops | bytes accessed | tf_op | source)
XLA Modules:
  0.0 67.4 jit_solution(15413102363547818577)
XLA Ops:
  0.0 66.7 %shard_map.64 = bf16[64,1024]{1,0:T(8,128)(2,1)S(1)} custom-call(bf16[512,1024]{1,0:T(8,128)(2,1)} %refs_0_.1, bf16[1024]{0:T(1024)(128)(2,1)} %refs_1_.1, bf16[1024,1408]{1,0:T(8,128)(2,1)} %refs_2_.1, bf16[1024,1408]{1,0:T(8,128)(2,1)} %refs_3_.1, bf16[1408,1024]{1,0:T(8,128)(2,1)} %refs_4_.1, bf16[1024]{0:T(1024)(128)(2,1)} %refs_5_.1), custom_call_target="tpu_custom_call" | custom-call | tf_op jit(solution)/shard_map/pallas_call | solution.py:383
  66.7 0.7 copy.8

commit v4 on v3

--- a/solution.py
+++ b/solution.py
@@ -16,6 +16,7 @@
 UNITS = sum(share if owners == WHOLE else share / 2 for share, owners in CHUNKS)
 FIRST_CUTS = (0, 1, 3, 5, 8)
 SECOND_CUTS = (0, 3, 7)
+HELD = (1, 0)
 VMEM_BYTES = 63 * 1024 * 1024 - 64 * 1024
 STEPS = (
     "P2 A0 P3 P4", "J2 J3 A1 J4", "P5 F0 L0 A2", "J5 P6 Y0 A3", "J6 P7 F1 L1", "Z0 A4 J7 P8",
@@ -64,17 +65,30 @@
 
 def semaphore_slots(total):
     n = len(CHUNKS)
-    keys = ["rows", "rest", "gain", "out_gain", "down"]
-    keys += [("weights", p) for p in range(len(FIRST_CUTS))]
+    done = ["rows", "rest", "gain", "out_gain", "down"]
+    done += [("weights", p) for p in range(len(FIRST_CUTS))]
+    done += [("dr", k, p) for k in range(2) for p in range(len(column_pieces(k, total)))]
+    keys = done + [("dr", k, 0) for k in range(2, n)]
     for k in range(n):
-        keys += [("dr", k, p) for p in range(len(column_pieces(k, total)))]
         keys += [("xr", k), ("hr", k), ("fr", k), ("zr", k)] + [("yr", k, h) for h in range(SLICES[k])]
     keys += [("qr", 0), ("qr", 1), "or", "os"]
-    for ring, depth in RINGS.items():
-        keys += [(ring, i) for i in range(depth)]
-    return {key: i for i, key in enumerate(keys)}
-
-
+    keys += [(ring, i) for ring in ("ds", "xs", "qs") for i in range(RINGS[ring])]
+    slots = {key: i for i, key in enumerate(key for key in keys if key not in REUSED)}
+    later = [(ring, i) for ring in ("hs", "cs", "fs", "ys", "zs") for i in range(RINGS[ring])]
+    slots.update({key: slots[taken] for key, taken in zip(later, done, strict=False)})
+    for key, first in REUSED.items():
+        slots[key] = slots[first]
+    return slots
+
+
+REUSED = {
+    ("dr", 6, 0): ("dr", 2, 0), ("dr", 7, 0): ("dr", 3, 0), ("dr", 8, 0): ("dr", 4, 0),
+    ("xr", 5): ("xr", 0), ("xr", 7): ("xr", 1), ("xr", 8): ("xr", 2),
+    ("hr", 6): ("hr", 0), ("hr", 8): ("hr", 1),
+    ("fr", 4): ("fr", 0), ("fr", 6): ("fr", 1), ("fr", 8): ("fr", 2),
+    ("yr", 3, 0): ("yr", 0, 0), ("yr", 5, 0): ("yr", 1, 0), ("yr", 6, 0): ("yr", 2, 0), ("yr", 8, 0): ("yr", 3, 0),
+    ("zr", 4): ("zr", 0),
+}
 RINGS = {"ds": 3, "xs": 4, "hs": 4, "cs": 2, "fs": 2, "ys": 3, "zs": 3, "qs": 1}
 
 
@@ -169,7 +183,7 @@
         cols = pl.ds(*column_pieces(k, 2 * units)[p])
         return send(part[k].at[oc, :, :, cols], prec[k].at[:, :, cols], "ds", sem("dr", k, p), core_peer)
 
-    leaving = {}
+    leaving, held = {}, []
 
     def combine(k, p, copy):
         with jax.named_scope(f"combine{k}"):
@@ -178,7 +192,12 @@
             part[k][c, :, :, cols] += prec[k][:, :, cols]
             if k not in leaving:
                 leaving[k] = slot_of("xs", lambda: wait_bytes(xrec[k], leaving[k]))
-            remote(part[k].at[c, ox, :, cols], xrec[k].at[:, cols], leaving[k], sem("xr", k), x_peer).start()
+            copy = remote(part[k].at[c, ox, :, cols], xrec[k].at[:, cols], leaving[k], sem("xr", k), x_peer)
+            if (k, p) == HELD:
+                pl.when(c == 0)(copy.start)
+                held.append(copy)
+            else:
+                copy.start()
 
     def activate(k, inv):
         with jax.named_scope(f"activate{k}"):
@@ -327,6 +346,8 @@
         q2 = send(sqp.at[c, ox], sqx, "qs", sem("qr", 1), x_peer)
     for p in range(len(column_pieces(1, 2 * units))):
         project(1, p)
+        if held:
+            pl.when(c != 0)(held.pop().start)
         waiting.append((1, p, to_core(1, p)))
         settle(1)
     settle(0)
@@ -406,7 +427,7 @@
             *[pltpu.VMEM((2, len(zs), sub, depth), f32) for _, sub, zs in layout],
             *[pltpu.VMEM((len(zs), sub, depth), f32) for _, sub, zs in layout],
             *[pltpu.VMEM((nz - 1, sub, depth), f32) for _, sub, _ in layout],
-            pltpu.SemaphoreType.DMA((len(semaphore_slots(2 * units)),)),
+            pltpu.SemaphoreType.DMA((1 + max(semaphore_slots(2 * units).values()),)),
         ],
         compiler_params=pltpu.CompilerParams(
             collective_id=0, has_side_effects=True, vmem_limit_bytes=VMEM_BYTES),

time: 67.5 us -> 67.1 us (level)
  no operation moved by 1% of the time
where the time goes in v4:
time: 67.1 us; the launch traced here: 66.8 us
  Pallas kernels  66.1 us (99%)
    pallas_call x1, Pallas kernels, fused_body(): pl.pallas_call(functools.partial(kernel, n_ra, width, layout), out_shape=...  66.1 us

profile of v4, /device:TPU:0, one launch (start us, length us, event | category | flops | bytes accessed | tf_op | source)
XLA Modules:
  0.0 66.8 jit_solution(15477166138388800570)
XLA Ops:
  0.0 66.1 %shard_map.64 = bf16[64,1024]{1,0:T(8,128)(2,1)S(1)} custom-call(bf16[512,1024]{1,0:T(8,128)(2,1)} %refs_0_.1, bf16[1024]{0:T(1024)(128)(2,1)} %refs_1_.1, bf16[1024,1408]{1,0:T(8,128)(2,1)} %refs_2_.1, bf16[1024,1408]{1,0:T(8,128)(2,1)} %refs_3_.1, bf16[1408,1024]{1,0:T(8,128)(2,1)} %refs_4_.1, bf16[1024]{0:T(1024)(128)(2,1)} %refs_5_.1), custom_call_target="tpu_custom_call" | custom-call | tf_op jit(solution)/shard_map/pallas_call | solution.py:404
  66.2 0.7 copy.8

commit v5 on v4

--- a/solution.py
+++ b/solution.py
@@ -19,9 +19,9 @@
 HELD = (1, 0)
 VMEM_BYTES = 63 * 1024 * 1024 - 64 * 1024
 STEPS = (
-    "P2 A0 P3 P4", "J2 J3 A1 J4", "P5 F0 L0 A2", "J5 P6 Y0 A3", "J6 P7 F1 L1", "Z0 A4 J7 P8",
-    "F2 L2 A5 J8", "Y1 F3 L3 A6", "Y2 F4 L4 A7", "F5 Y3 L5 A8", "Z1 F6 F7 Y4", "L6 F8 L7 Y5",
-    "Z2 L8 Z3 Y6", "Y7 Z4 Y8 Z5", "Z6 Z7 Z8",
+    "P2 A0 P3 P4", "J2 J3 A1 J4", "P5 F0 L0 A2", "J5 P6 Y0 A3", "P7 F1 L1 Z0", "A4 J6 J7 P8",
+    "F2 L2 A5 J8", "Y1 F3 L3 F4", "Y2 L4 A6 A7", "F5 Y3 L5 A8", "Z1 F6 F7 Y4", "L6 F8 L7 Y5",
+    "Z2 L8 Z3 Y6", "Y7 Y8 Z4 Z5", "Z6 Z7 Z8",
 )
 SLICES = (1, 1, 1, 1, 1, 2, 2, 2, 2)
 
@@ -85,7 +85,7 @@
     ("dr", 6, 0): ("dr", 2, 0), ("dr", 7, 0): ("dr", 3, 0), ("dr", 8, 0): ("dr", 4, 0),
     ("xr", 5): ("xr", 0), ("xr", 7): ("xr", 1), ("xr", 8): ("xr", 2),
     ("hr", 6): ("hr", 0), ("hr", 8): ("hr", 1),
-    ("fr", 4): ("fr", 0), ("fr", 6): ("fr", 1), ("fr", 8): ("fr", 2),
+    ("fr", 5): ("fr", 0), ("fr", 6): ("fr", 1), ("fr", 8): ("fr", 2),
     ("yr", 3, 0): ("yr", 0, 0), ("yr", 5, 0): ("yr", 1, 0), ("yr", 6, 0): ("yr", 2, 0), ("yr", 8, 0): ("yr", 3, 0),
     ("zr", 4): ("zr", 0),
 }

time: 67.1 us -> 67.1 us (level)
  no operation moved by 1% of the time
where the time goes in v5:
time: 67.1 us; the launch traced here: 66.8 us
  Pallas kernels  66.1 us (99%)
    pallas_call x1, Pallas kernels, fused_body(): pl.pallas_call(functools.partial(kernel, n_ra, width, layout), out_shape=...  66.1 us

profile of v5, /device:TPU:0, one launch (start us, length us, event | category | flops | bytes accessed | tf_op | source)
XLA Modules:
  0.0 66.8 jit_solution(9750982364150580130)
XLA Ops:
  0.0 66.1 %shard_map.64 = bf16[64,1024]{1,0:T(8,128)(2,1)S(1)} custom-call(bf16[512,1024]{1,0:T(8,128)(2,1)} %refs_0_.1, bf16[1024]{0:T(1024)(128)(2,1)} %refs_1_.1, bf16[1024,1408]{1,0:T(8,128)(2,1)} %refs_2_.1, bf16[1024,1408]{1,0:T(8,128)(2,1)} %refs_3_.1, bf16[1408,1024]{1,0:T(8,128)(2,1)} %refs_4_.1, bf16[1024]{0:T(1024)(128)(2,1)} %refs_5_.1), custom_call_target="tpu_custom_call" | custom-call | tf_op jit(solution)/shard_map/pallas_call | solution.py:404
  66.2 0.7 copy.8

commit v6 on v5

--- a/solution.py
+++ b/solution.py
@@ -329,7 +329,7 @@
             with jax.named_scope("enter"):
                 pl.semaphore_wait(barrier, len(peers))
         waiting.append((0, p, to_core(0, p)))
-        settle(1 if p == 2 else 2)
+        settle(1 if p in (2, 3) else 2)
     with jax.named_scope("rest"):
         whole_tok.wait()
     q1 = squares()
@@ -339,16 +339,16 @@
             at = pl.ds(d * own, own)
             xs[at, :] = tok[at, :].astype(jnp.float32) * gain
         fill(1)
-    settle(0)
-    with jax.named_scope("share"):
-        q1.wait_recv()
-        sqp[c] += sqd[...]
-        q2 = send(sqp.at[c, ox], sqx, "qs", sem("qr", 1), x_peer)
     for p in range(len(column_pieces(1, 2 * units))):
         project(1, p)
         if held:
             pl.when(c != 0)(held.pop().start)
         waiting.append((1, p, to_core(1, p)))
+        if p == 1:
+            with jax.named_scope("share"):
+                q1.wait_recv()
+                sqp[c] += sqd[...]
+                q2 = send(sqp.at[c, ox], sqx, "qs", sem("qr", 1), x_peer)
         settle(1)
     settle(0)
     for k in range(2, n):

time: 67.1 us -> 67.3 us (level)
  no operation moved by 1% of the time
where the time goes in v6:
time: 67.3 us; the launch traced here: 67.1 us
  Pallas kernels  66.5 us (99%)
    pallas_call x1, Pallas kernels, fused_body(): pl.pallas_call(functools.partial(kernel, n_ra, width, layout), out_shape=...  66.5 us

profile of v6, /device:TPU:0, one launch (start us, length us, event | category | flops | bytes accessed | tf_op | source)
XLA Modules:
  0.0 67.1 jit_solution(1730926773713627497)
XLA Ops:
  0.0 66.5 %shard_map.64 = bf16[64,1024]{1,0:T(8,128)(2,1)S(1)} custom-call(bf16[512,1024]{1,0:T(8,128)(2,1)} %refs_0_.1, bf16[1024]{0:T(1024)(128)(2,1)} %refs_1_.1, bf16[1024,1408]{1,0:T(8,128)(2,1)} %refs_2_.1, bf16[1024,1408]{1,0:T(8,128)(2,1)} %refs_3_.1, bf16[1408,1024]{1,0:T(8,128)(2,1)} %refs_4_.1, bf16[1024]{0:T(1024)(128)(2,1)} %refs_5_.1), custom_call_target="tpu_custom_call" | custom-call | tf_op jit(solution)/shard_map/pallas_call | solution.py:404
  66.5 0.7 copy.8
